TPU v7x, 32 devices: a whole 2x2x4 slice. The times are simulated.
32 devices in a mesh: kv: 8 (over z, y), tp: 4 (over x, core).
Axes of the slice: x: 2, y: 2, z: 4, core: 2. Of those that a mesh axis runs over, the one named last changes fastest.
Arguments:
- residual_in: bfloat16 [64, 2048], P(None, ('kv', 'tp')), may hold values from -14 to 14
- delta_state: float32 [64, 32, 128, 128], P('kv', 'tp'), may hold values from -1 to 1
- norm_gain_first: float32 [2048], P('kv'), may hold values from 0.1 to 1.9
- gate_first: bfloat16 [2048, 5632], P('kv', 'tp'), may hold values from -0.125 to 0.125
- up_first: bfloat16 [2048, 5632], P('kv', 'tp'), may hold values from -0.125 to 0.125
- down_first: bfloat16 [5632, 2048], P('tp', 'kv'), may hold values from -0.15625 to 0.15625
- norm_gain_mixer: float32 [2048], P('kv'), may hold values from 0.1 to 1.9
- query_weight: bfloat16 [2048, 2048], P('kv', 'tp'), may hold values from -0.125 to 0.125
- key_weight: bfloat16 [2048, 2048], P('kv', 'tp'), may hold values from -0.125 to 0.125
- value_weight: bfloat16 [2048, 4096], P('kv', 'tp'), may hold values from -0.125 to 0.125
- output_gate_weight: bfloat16 [2048, 4096], P('kv', 'tp'), may hold values from -0.125 to 0.125
- beta_weight: bfloat16 [2048, 32], P('kv'), may hold values from -0.125 to 0.125
- decay_weight: bfloat16 [2048, 32], P('kv'), may hold values from -0.125 to 0.125
- decay_rate: float32 [32], P('tp'), may hold values from -2.3 to 1.1
- decay_bias: float32 [32], P('tp'), may hold values from -1 to 1
- head_gain: float32 [128], replicated, may hold values from 0.1 to 1.9
- out_weight: bfloat16 [4096, 2048], P('tp', 'kv'), may hold values from -0.125 to 0.125
- norm_gain_second: float32 [2048], P('kv'), may hold values from 0.1 to 1.9
- gate_second: bfloat16 [2048, 5632], P('kv', 'tp'), may hold values from -0.125 to 0.125
- up_second: bfloat16 [2048, 5632], P('kv', 'tp'), may hold values from -0.125 to 0.125
- down_second: bfloat16 [5632, 2048], P('tp', 'kv'), may hold values from -0.15625 to 0.15625
Outputs:
- residual_out: bfloat16 [64, 2048], P(None, ('kv', 'tp'))
- delta_state_out: float32 [64, 32, 128, 128], P('kv', 'tp')
All inputs are finite; a program needn't handle non-finite values.
Results may differ from a plain program's by a relative error of at most 0.03.
Values may be sent and summed in bfloat16 or wider, within the bound.
A program may use at most 64 MiB of HBM per device.

v0:
```python
import jax
import jax.numpy as jnp
from jax import lax
from jax.sharding import PartitionSpec as P

D = 2048
epsilon = 1e-06


def activate(summed, square_sums, hidden_cols):
    rowscale = lax.rsqrt(square_sums / D + epsilon)[:, None]
    gate_act = summed[:, :hidden_cols] * rowscale
    up_act = summed[:, hidden_cols:] * rowscale
    return (jax.nn.silu(gate_act) * up_act).astype(jnp.bfloat16)


def feed_forward(residual, norm_gain, gate_weight, up_weight, down_weight, finish):
    as_float = residual.astype(jnp.float32)
    squares = jnp.sum(as_float * as_float, axis=1)
    scaled = (as_float * norm_gain).astype(jnp.bfloat16)
    joined = jnp.concatenate([gate_weight, up_weight], axis=1)
    partial_value = jnp.dot(scaled, joined, preferred_element_type=jnp.float32)
    hidden_cols = gate_weight.shape[1]
    summed, square_sums = (
        lax.psum(partial_value.astype(jnp.bfloat16), "kv").astype(jnp.float32),
        lax.psum(squares.astype(jnp.bfloat16), "kv").astype(jnp.float32),
    )
    hidden = activate(summed, square_sums, hidden_cols)
    projected = jnp.dot(hidden, down_weight, preferred_element_type=jnp.float32).astype(
        jnp.bfloat16
    )
    if finish:
        col_count = residual.shape[1] // lax.axis_size("tp")
        own_cols = lax.dynamic_slice_in_dim(
            as_float, lax.axis_index("tp") * col_count, col_count, 1
        )
        branch = lax.psum_scatter(projected, "tp", scatter_dimension=1, tiled=True).astype(
            jnp.float32
        )
        return (own_cols + 0.5 * branch).astype(jnp.bfloat16)
    branch = lax.psum(projected, "tp").astype(jnp.float32)
    return (as_float + 0.5 * branch).astype(jnp.bfloat16)


def unit_heads(projected, head_size):
    activated = jax.nn.silu(projected).reshape(projected.shape[0], -1, head_size)
    return activated * lax.rsqrt(jnp.sum(activated * activated, axis=-1, keepdims=True) + epsilon)


def delta_step(old_state, key_rows, queries, values, beta_gate, decay_gate):
    faded_state = old_state * decay_gate[:, :, None, None]
    predicted = jnp.einsum("rhab,rha->rhb", faded_state, key_rows, precision=lax.Precision.HIGHEST)
    correction = beta_gate[:, :, None] * (values - predicted)
    updated = faded_state + key_rows[:, :, :, None] * correction[:, :, None, :]
    reading = jnp.einsum("rhab,rha->rhb", updated, queries, precision=lax.Precision.HIGHEST)
    return (updated, reading)


def token_mixer(
    residual,
    norm_gain,
    query_weight,
    key_weight,
    value_weight,
    output_gate_weight,
    beta_weight,
    decay_weight,
    decay_rate,
    decay_bias,
    head_gain,
    out_weight,
    old_state,
):
    as_float = residual.astype(jnp.float32)
    squares = jnp.sum(as_float * as_float, axis=1)
    scaled = (as_float * norm_gain).astype(jnp.bfloat16)
    joined = jnp.concatenate([query_weight, key_weight, value_weight, output_gate_weight], axis=1)
    partial_value = jnp.dot(scaled, joined, preferred_element_type=jnp.float32)
    heads_dev = decay_rate.shape[0]
    head_start = lax.axis_index("tp") * heads_dev
    gate_cols = jnp.concatenate(
        [
            lax.dynamic_slice_in_dim(beta_weight, head_start, heads_dev, 1),
            lax.dynamic_slice_in_dim(decay_weight, head_start, heads_dev, 1),
        ],
        axis=1,
    )
    gate_part = jnp.dot(scaled, gate_cols, preferred_element_type=jnp.float32)
    row_count = old_state.shape[0]
    square_sums = lax.psum(squares, "kv")
    square_sums = lax.dynamic_slice_in_dim(
        square_sums, lax.axis_index("kv") * row_count, row_count, 0
    )
    summed, gate_summed = (
        lax.psum_scatter(
            partial_value.astype(jnp.bfloat16), "kv", scatter_dimension=0, tiled=True
        ).astype(jnp.float32),
        lax.psum_scatter(
            gate_part.astype(jnp.bfloat16), "kv", scatter_dimension=0, tiled=True
        ).astype(jnp.float32),
    )
    rowscale = lax.rsqrt(square_sums / D + epsilon)[:, None]
    summed = summed * rowscale
    gate_summed = gate_summed * rowscale
    head_size = old_state.shape[2]
    key_cols = query_weight.shape[1]
    value_cols = value_weight.shape[1]
    repeat_count = heads_dev // (key_cols // head_size)
    queries = jnp.repeat(
        unit_heads(summed[:, :key_cols], head_size) * head_size ** (-0.5), repeat_count, axis=1
    )
    key_rows = jnp.repeat(
        unit_heads(summed[:, key_cols : 2 * key_cols], head_size), repeat_count, axis=1
    )
    values = jax.nn.silu(summed[:, 2 * key_cols : 2 * key_cols + value_cols]).reshape(
        row_count, heads_dev, head_size
    )
    out_gate = jax.nn.silu(summed[:, 2 * key_cols + value_cols :]).reshape(
        row_count, heads_dev, head_size
    )
    beta_gate = jax.nn.sigmoid(gate_summed[:, :heads_dev])
    decay_gate = jnp.exp(
        -jnp.exp(decay_rate)[None, :]
        * jax.nn.softplus(gate_summed[:, heads_dev:] + decay_bias[None, :])
    )
    new_state, reading = delta_step(old_state, key_rows, queries, values, beta_gate, decay_gate)
    normed = reading * lax.rsqrt(jnp.mean(reading * reading, axis=-1, keepdims=True) + epsilon)
    normed = (
        (normed * head_gain * out_gate)
        .reshape(row_count, heads_dev * head_size)
        .astype(jnp.bfloat16)
    )
    projected = jnp.dot(
        lax.all_gather(normed, "kv", axis=0, tiled=True),
        out_weight,
        preferred_element_type=jnp.float32,
    ).astype(jnp.bfloat16)
    branch = lax.psum(projected, "tp").astype(jnp.float32)
    return ((as_float + branch).astype(jnp.bfloat16), new_state)


def body(
    residual_in,
    delta_state,
    norm_gain_first,
    gate_first,
    up_first,
    down_first,
    norm_gain_mixer,
    query_weight,
    key_weight,
    value_weight,
    output_gate_weight,
    beta_weight,
    decay_weight,
    decay_rate,
    decay_bias,
    head_gain,
    out_weight,
    norm_gain_second,
    gate_second,
    up_second,
    down_second,
):
    columns = lax.all_gather(residual_in, "tp", axis=1, tiled=True)
    after_first = feed_forward(columns, norm_gain_first, gate_first, up_first, down_first, False)
    after_mixer, new_state = token_mixer(
        after_first,
        norm_gain_mixer,
        query_weight,
        key_weight,
        value_weight,
        output_gate_weight,
        beta_weight,
        decay_weight,
        decay_rate,
        decay_bias,
        head_gain,
        out_weight,
        delta_state,
    )
    residual_out = feed_forward(
        after_mixer, norm_gain_second, gate_second, up_second, down_second, True
    )
    return (residual_out, new_state)


def solution(mesh):
    placed = (
        P(None, ("kv", "tp")),
        P("kv", "tp", None, None),
        P("kv"),
        P("kv", "tp"),
        P("kv", "tp"),
        P("tp", "kv"),
        P("kv"),
        P("kv", "tp"),
        P("kv", "tp"),
        P("kv", "tp"),
        P("kv", "tp"),
        P("kv", None),
        P("kv", None),
        P("tp"),
        P("tp"),
        P(),
        P("tp", "kv"),
        P("kv"),
        P("kv", "tp"),
        P("kv", "tp"),
        P("tp", "kv"),
    )
    return jax.shard_map(
        body,
        mesh=mesh,
        in_specs=placed,
        out_specs=(P(None, ("kv", "tp")), P("kv", "tp", None, None)),
        check_vma=False,
    )
```

profile of v0, /device:TPU:0, one launch (start us, length us, event | category | flops | bytes accessed | tf_op | source)
XLA Modules:
  0.0 322.3 jit_solution(16253293188831210375)
XLA Ops:
  7.2 0.9 copy.27
  8.1 6.2 %all_gather.6 = bf16[64,256]{0,1:T(8,128)(2,1)S(1)} all-gather(bf16[64,64]{0,1:T(8,128)(2,1)S(1)} %copy.27), channel_id=1, replica_groups=mesh['kv'=8,'tp'=4] {'tp'}, dimensions={1}, use_global_device_ids=true | all-gather | bytes 40960 | tf_op jit(solution)/shard_map/all_gather | solution.py:165
  14.3 0.1 copy.28
  14.4 2.6 convolution_convert_fusion.2
  17.0 0.0 reduce-scatter.5.cloned.1.call-start
  17.1 0.1 fusion.27
  17.2 22.4 %psum.50 = bf16[64]{0:T(256)(128)(2,1)S(1)} all-reduce(bf16[64]{0:T(256)(128)(2,1)S(1)} %fusion.27), channel_id=1, replica_groups=mesh['kv'=8,'tp'=4] {'kv'}, use_global_device_ids=true, to_apply=%region_2.0 | all-reduce | flops 64 | bytes 256 | tf_op jit(solution)/shard_map/psum | solution.py:26
  39.6 1.2 dynamic-slice
  41.5 0.7 constant_dynamic-slice_fusion
  42.2 0.7 exponential_negate_fusion
  42.9 47.6 %all-reduce.4.cloned.1.call-done = bf16[64,2816]{1,0:T(8,128)(2,1)} async-done(((bf16[64,2816]{1,0:T(8,128)(2,1)}), bf16[64,2816]{1,0:T(8,128)(2,1)}) %all-reduce.4.cloned.1.call-update) | async-done | bytes 360464 | tf_op jit(solution)/shard_map/psum | solution.py:25
  90.5 1.0 convert_element_type.96
  91.5 0.3 convolution_convert_fusion.5
  91.9 10.3 %psum.51 = bf16[64,256]{1,0:T(8,128)(2,1)S(1)} all-reduce(bf16[64,256]{1,0:T(8,128)(2,1)S(1)} %convolution_convert_fusion.5), channel_id=1, replica_groups=mesh['kv'=8,'tp'=4] {'tp'}, use_global_device_ids=true, to_apply=%region_3.4 | all-reduce | flops 16384 | bytes 65536 | tf_op jit(solution)/shard_map/psum | solution.py:41
  102.1 0.1 fusion.30
  102.3 1.1 convolution_convert_fusion.1
  103.5 0.0 all-reduce.6.cloned.1.call-start
  103.5 19.7 %psum.52 = f32[64]{0:T(128)S(1)} all-reduce(f32[64]{0:T(128)S(1)} %get-tuple-element.4), channel_id=1, replica_groups=mesh['kv'=8,'tp'=4] {'kv'}, use_global_device_ids=true, to_apply=%region_6.7 | all-reduce | flops 64 | bytes 512 | tf_op jit(solution)/shard_map/psum | solution.py:90
  123.3 0.1 convolution_convert_fusion.6
  123.4 33.1 %all-reduce = bf16[64,16]{1,0:T(8,128)(2,1)S(1)} all-reduce(bf16[64,16]{1,0:T(8,128)(2,1)S(1)} %convolution_convert_fusion.6), channel_id=2, replica_groups=mesh['kv'=8,'tp'=4] {'kv'}, use_global_device_ids=true, to_apply=%region_4.5.clone | all-reduce | flops 1024 | bytes 4096
  156.5 0.1 add_rsqrt_fusion.4
  156.5 0.1 convert_multiply_fusion.5
  156.6 0.1 add_divide_fusion
  156.7 0.1 copy.30
  156.8 8.5 %reduce-scatter.5.cloned.1.call-done = bf16[8,3072]{1,0:T(8,128)(2,1)} async-done(((bf16[64,3072]{1,0:T(8,128)(2,1)}), bf16[8,3072]{1,0:T(8,128)(2,1)}) %reduce-scatter.5.cloned.1.call-update) | async-done | bytes 49168 | tf_op jit(solution)/shard_map/reduce_scatter | solution.py:95
  165.2 1.0 convert_multiply_fusion
  166.3 0.1 fusion.42
  166.4 0.1 fusion.43
  166.5 5.8 %fusion = f32[8,8,1,128]{3,2,1,0:T(1,128)S(1)} fusion(f32[8,8,128,1]{2,3,1,0:T(1,128)S(1)} %bitcast.57, f32[8,8,128,128]{3,2,1,0:T(8,128)} %param.22, f32[8,8]{1,0:T(8,128)S(1)} %get-tuple-element.11), kind=kOutput, calls=%fused_computation.1 | convolution fusion | flops 13631488 | bytes 4260096 | tf_op jit(solution)/shard_map/rhab,rha->rhb/dot_general | solution.py:52
  172.3 0.1 fusion.37
  172.4 1.5 multiply_add_fusion
  174.0 2.0 copy-done.2
  176.0 3.6 %fusion.59 = f32[8,8,1,128]{3,2,1,0:T(1,128)S(1)} fusion(f32[8,8,128,128]{3,2,1,0:T(8,128)S(1)} %multiply_add_fusion, f32[8,8,128,1]{2,3,1,0:T(1,128)S(1)} %bitcast.60), kind=kOutput, calls=%fused_computation.96 | convolution fusion | flops 12582912 | bytes 4259840 | tf_op jit(solution)/shard_map/rhab,rha->rhb/dot_general | solution.py:55
  179.7 0.1 fusion.35
  179.8 0.1 fusion.45
  179.9 30.6 %all_gather.7 = bf16[64,1024]{1,0:T(8,128)(2,1)S(1)} all-gather(bf16[8,1024]{1,0:T(8,128)(2,1)S(1)} %fusion.45), channel_id=1, replica_groups=mesh['kv'=8,'tp'=4] {'kv'}, dimensions={0}, use_global_device_ids=true | all-gather | bytes 147456 | tf_op jit(solution)/shard_map/all_gather | solution.py:134
  210.5 0.2 convolution_convert_fusion.4
  210.8 10.3 %psum.53 = bf16[64,256]{1,0:T(8,128)(2,1)S(1)} all-reduce(bf16[64,256]{1,0:T(8,128)(2,1)S(1)} %convolution_convert_fusion.4), channel_id=1, replica_groups=mesh['kv'=8,'tp'=4] {'tp'}, use_global_device_ids=true, to_apply=%region_11.12 | all-reduce | flops 16384 | bytes 65536 | tf_op jit(solution)/shard_map/psum | solution.py:138
  221.1 1.1 convolution_convert_fusion
  222.3 0.1 fusion.32
  222.4 19.7 %psum.55 = bf16[64]{0:T(256)(128)(2,1)S(1)} all-reduce(bf16[64]{0:T(256)(128)(2,1)S(1)} %get-tuple-element.9), channel_id=1, replica_groups=mesh['kv'=8,'tp'=4] {'kv'}, use_global_device_ids=true, to_apply=%region_14.15 | all-reduce | flops 64 | bytes 256 | tf_op jit(solution)/shard_map/psum | solution.py:26
  242.1 51.1 %all-reduce.6.cloned.1.call-done = bf16[64,2816]{1,0:T(8,128)(2,1)} async-done(((bf16[64,2816]{1,0:T(8,128)(2,1)}), bf16[64,2816]{1,0:T(8,128)(2,1)}) %all-reduce.6.cloned.1.call-update) | async-done | bytes 360464 | tf_op jit(solution)/shard_map/psum | solution.py:25
  293.2 1.0 convert_element_type.117
  294.3 0.3 convolution_convert_fusion.3
  294.6 0.7 copy.37
  295.3 19.0 %reduce-scatter.7.cloned.1.call-done = bf16[64,64]{1,0:T(8,128)(2,1)} async-done(((bf16[256,64]{1,0:T(8,128)(2,1)}), bf16[64,64]{1,0:T(8,128)(2,1)}) %reduce-scatter.7.cloned.1.call-update) | async-done | bytes 8208
  314.3 0.8 copy.38
  315.1 0.7 add_convert_fusion
  (44 shorter events, 0.3 us)
Async XLA Ops:
  7.2 84.4 %copy-start = (bf16[1408,256]{1,0:T(8,128)(2,1)S(1)}, bf16[1408,256]{1,0:T(8,128)(2,1)}, u32[]{:S(2)}) copy-start(bf16[1408,256]{1,0:T(8,128)(2,1)} %param.26) | copy-start | bytes 2162692
  7.2 83.3 %all-reduce.4.cloned.1.call-start = ((), (), s32[]{:S(2)}) async-start(), calls=%async_computation.2 | async-start | bytes 720896 | tf_op jit(solution)/shard_map/psum | solution.py:25
  14.4 87.9 %copy-start.9 = (bf16[256,1024]{1,0:T(8,128)(2,1)S(1)}, bf16[256,1024]{1,0:T(8,128)(2,1)}, u32[]{:S(2)}) copy-start(bf16[256,1024]{1,0:T(8,128)(2,1)} %param.31) | copy-start | bytes 1572868
  14.4 87.9 %copy-start.10 = (bf16[256,1024]{1,0:T(8,128)(2,1)S(1)}, bf16[256,1024]{1,0:T(8,128)(2,1)}, u32[]{:S(2)}) copy-start(bf16[256,1024]{1,0:T(8,128)(2,1)} %param.30) | copy-start | bytes 1572868
  14.4 87.9 %copy-start.11 = (bf16[256,512]{1,0:T(8,128)(2,1)S(1)}, bf16[256,512]{1,0:T(8,128)(2,1)}, u32[]{:S(2)}) copy-start(bf16[256,512]{1,0:T(8,128)(2,1)} %param.29) | copy-start | bytes 786436
  14.4 87.9 %copy-start.12 = (bf16[256,512]{1,0:T(8,128)(2,1)S(1)}, bf16[256,512]{1,0:T(8,128)(2,1)}, u32[]{:S(2)}) copy-start(bf16[256,512]{1,0:T(8,128)(2,1)} %param.28) | copy-start | bytes 786436
  14.4 87.9 %copy-start.13 = (f32[256]{0:T(256)S(1)}, f32[256]{0:T(256)}, u32[]{:S(2)}) copy-start(f32[256]{0:T(256)} %param.27) | copy-start | bytes 3076
  17.0 148.2 %reduce-scatter.5.cloned.1.call-start = ((), (), s32[]{:S(2)}) async-start(), calls=%async_computation.3 | async-start | bytes 442368 | tf_op jit(solution)/shard_map/reduce_scatter | solution.py:95
  91.9 64.7 %copy-start.5 = (f32[8]{0:T(128)S(1)}, f32[8]{0:T(128)}, u32[]{:S(2)}) copy-start(f32[8]{0:T(128)} %param.35) | copy-start | bytes 100
  103.5 189.7 %all-reduce.6.cloned.1.call-start = ((), (), s32[]{:S(2)}) async-start(), calls=%async_computation.4 | async-start | bytes 720896 | tf_op jit(solution)/shard_map/psum | solution.py:25
  165.2 7.2 %copy-start.1 = (f32[8,8,128,128]{3,2,1,0:T(8,128)S(1)}, f32[8,8,128,128]{3,2,1,0:T(8,128)}, u32[]{:S(2)}) copy-start(f32[8,8,128,128]{3,2,1,0:T(8,128)} %param.22) | copy-start | bytes 12582916
  173.9 2.1 copy-start.2
  173.9 5.9 %copy-start.4 = (f32[128]{0:T(128)S(1)}, f32[128]{0:T(128)}, u32[]{:S(2)}) copy-start(f32[128]{0:T(128)} %param.36) | copy-start | bytes 1540
  173.9 36.6 %copy-start.3 = (bf16[1024,256]{1,0:T(8,128)(2,1)S(1)}, bf16[1024,256]{1,0:T(8,128)(2,1)}, u32[]{:S(2)}) copy-start(bf16[1024,256]{1,0:T(8,128)(2,1)} %param.37) | copy-start | bytes 1572868
  173.9 47.1 %copy-start.6 = (bf16[256,1408]{1,0:T(8,128)(2,1)S(1)}, bf16[256,1408]{1,0:T(8,128)(2,1)}, u32[]{:S(2)}) copy-start(bf16[256,1408]{1,0:T(8,128)(2,1)} %param.40) | copy-start | bytes 2162692
  174.0 47.1 %copy-start.7 = (bf16[256,1408]{1,0:T(8,128)(2,1)S(1)}, bf16[256,1408]{1,0:T(8,128)(2,1)}, u32[]{:S(2)}) copy-start(bf16[256,1408]{1,0:T(8,128)(2,1)} %param.39) | copy-start | bytes 2162692
  174.0 47.1 %copy-start.14 = (f32[256]{0:T(256)S(1)}, f32[256]{0:T(256)}, u32[]{:S(2)}) copy-start(f32[256]{0:T(256)} %param.38) | copy-start | bytes 3076
  179.7 114.5 %copy-start.8 = (bf16[1408,256]{1,0:T(8,128)(2,1)S(1)}, bf16[1408,256]{1,0:T(8,128)(2,1)}, u32[]{:S(2)}) copy-start(bf16[1408,256]{1,0:T(8,128)(2,1)} %param.41) | copy-start | bytes 2162692
  222.2 92.1 %reduce-scatter.7.cloned.1.call-start = ((), (), s32[]{:S(2)}) async-start(), calls=%async_computation.5 | async-start | bytes 81920
Sparse Core Ops, SparseCore 0:
  17.1 73.3 all-reduce.3
  103.6 61.5 reduce-scatter.4
  222.3 70.8 all-reduce.5
  295.5 18.7 reduce-scatter.6
where the time goes:
time: 323 us; the launch traced here: 322 us
  blocking collectives  152 us (47%)
  waiting for transfers between devices  126 us (39%)
  matrix products  15.2 us (5%)
  between operations  14.7 us (5%)
  other arithmetic  6.96 us (2%)
  local copies, waits for them, and re-layouts  6.68 us (2%)
    psum x2, waiting for transfers between devices, feed_forward(): lax.psum(partial_value.astype(jnp.bfloat16), 'kv').astype(jnp.float32)  98.7 us
    psum x2, blocking collectives, feed_forward(): lax.psum(squares.astype(jnp.bfloat16), 'kv').astype(jnp.float32)  42.1 us
    unnamed x1, blocking collectives  33.1 us
    all_gather x1, blocking collectives, token_mixer(): lax.all_gather(normed, 'kv', axis=0, tiled=True)  30.6 us
    psum x1, blocking collectives, token_mixer(): square_sums = lax.psum(squares, 'kv')  19.7 us
    unnamed x5, waiting for transfers between devices  19.1 us
    psum x1, blocking collectives, feed_forward(): branch = lax.psum(projected, 'tp').astype(jnp.float32)  10.3 us
    psum x1, blocking collectives, token_mixer(): branch = lax.psum(projected, 'tp').astype(jnp.float32)  10.3 us
  transfers between devices with their start and end apart: 4, of which 4 were waited for; matrix products, arithmetic and copies ran while one was open for 1% of the time, Pallas kernels for 0%

commit v1 on v0

--- a/solution.py
+++ b/solution.py
@@ -23,7 +23,7 @@
     hidden_cols = gate_weight.shape[1]
     summed, square_sums = (
         lax.psum(partial_value.astype(jnp.bfloat16), "kv").astype(jnp.float32),
-        lax.psum(squares.astype(jnp.bfloat16), "kv").astype(jnp.float32),
+        jnp.sum(lax.all_gather(squares.astype(jnp.bfloat16), "kv"), axis=0).astype(jnp.float32),
     )
     hidden = activate(summed, square_sums, hidden_cols)
     projected = jnp.dot(hidden, down_weight, preferred_element_type=jnp.float32).astype(

time: 323 us -> 341 us (1.056)
  waiting for transfers between devices: 126 us -> 143 us
    psum x2 -> x0, blocking collectives: 42.1 us -> none  [feed_forward(): lax.psum(squares.astype(jnp.bfloat16), 'kv').astype(jnp.float32)]
    unnamed x1 -> x3, blocking collectives: 33.1 us -> 75 us
    reduce_scatter x1, waiting for transfers between devices: 8.47 us -> 26.2 us  [token_mixer(): lax.psum_scatter(partial_value.astype(jnp.bfloat16), 'kv', scatter_dimens...]
where the time goes in v1:
time: 341 us; the launch traced here: 340 us
  blocking collectives  152 us (45%)
  waiting for transfers between devices  143 us (42%)
  between operations  15.4 us (5%)
  matrix products  15.2 us (4%)
  local copies, waits for them, and re-layouts  7.45 us (2%)
  other arithmetic  7 us (2%)
    psum x2, waiting for transfers between devices, feed_forward(): lax.psum(partial_value.astype(jnp.bfloat16), 'kv').astype(jnp.float32)  97.5 us
    unnamed x3, blocking collectives  75 us
    all_gather x1, blocking collectives, token_mixer(): lax.all_gather(normed, 'kv', axis=0, tiled=True)  30.6 us
    reduce_scatter x1, waiting for transfers between devices, token_mixer(): lax.psum_scatter(partial_value.astype(jnp.bfloat16), 'kv', scatter_dimens...  26.2 us
    psum x1, blocking collectives, token_mixer(): square_sums = lax.psum(squares, 'kv')  19.7 us
    unnamed x5, waiting for transfers between devices  19.1 us
    psum x1, blocking collectives, token_mixer(): branch = lax.psum(projected, 'tp').astype(jnp.float32)  10.3 us
    psum x1, blocking collectives, feed_forward(): branch = lax.psum(projected, 'tp').astype(jnp.float32)  10.3 us
  transfers between devices with their start and end apart: 4, of which 4 were waited for; matrix products, arithmetic and copies ran while one was open for 1% of the time, Pallas kernels for 0%

profile of v1, /device:TPU:0, one launch (start us, length us, event | category | flops | bytes accessed | tf_op | source)
XLA Modules:
  0.0 340.1 jit_solution(14515264399025347004)
XLA Ops:
  7.2 0.9 copy.33
  8.1 6.2 %all_gather.14 = bf16[64,256]{0,1:T(8,128)(2,1)S(1)} all-gather(bf16[64,64]{0,1:T(8,128)(2,1)S(1)} %copy.33), channel_id=1, replica_groups=mesh['kv'=8,'tp'=4] {'tp'}, dimensions={1}, use_global_device_ids=true | all-gather | bytes 40960 | tf_op jit(solution)/shard_map/all_gather | solution.py:165
  14.3 0.1 copy.34
  14.4 2.6 convolution_convert_fusion.2
  17.1 0.7 exponential_negate_fusion
  17.7 0.1 fusion.27
  17.9 1.3 fusion.59
  19.8 0.2 dynamic-update-slice
  20.1 22.2 %all-reduce = bf16[512]{0:T(512)(128)(2,1)S(1)} all-reduce(bf16[512]{0:T(512)(128)(2,1)S(1)} %dynamic-update-slice), channel_id=2, replica_groups=mesh['kv'=8,'tp'=4] {'kv'}, use_global_device_ids=true, to_apply=%add | all-reduce | flops 512 | bytes 2048
  42.3 0.1 reshape.87
  43.0 0.7 constant_dynamic-slice_fusion
  43.8 46.8 %all-reduce.6.cloned.1.call-done = bf16[64,2816]{1,0:T(8,128)(2,1)} async-done(((bf16[64,2816]{1,0:T(8,128)(2,1)}), bf16[64,2816]{1,0:T(8,128)(2,1)}) %all-reduce.6.cloned.1.call-update) | async-done | bytes 360464 | tf_op jit(solution)/shard_map/psum | solution.py:25
  90.5 1.0 convert_element_type.128
  91.6 0.3 convolution_convert_fusion.5
  91.9 10.3 %psum.36 = bf16[64,256]{1,0:T(8,128)(2,1)S(1)} all-reduce(bf16[64,256]{1,0:T(8,128)(2,1)S(1)} %convolution_convert_fusion.5), channel_id=1, replica_groups=mesh['kv'=8,'tp'=4] {'tp'}, use_global_device_ids=true, to_apply=%region_3.4 | all-reduce | flops 16384 | bytes 65536 | tf_op jit(solution)/shard_map/psum | solution.py:41
  102.2 0.1 fusion.30
  102.3 19.7 %psum.37 = f32[64]{0:T(128)S(1)} all-reduce(f32[64]{0:T(128)S(1)} %get-tuple-element.4), channel_id=1, replica_groups=mesh['kv'=8,'tp'=4] {'kv'}, use_global_device_ids=true, to_apply=%region_6.7 | all-reduce | flops 64 | bytes 512 | tf_op jit(solution)/shard_map/psum | solution.py:90
  122.0 1.1 convolution_convert_fusion.1
  123.2 0.1 convolution_convert_fusion.6
  123.4 33.1 %all-reduce.2 = bf16[64,16]{1,0:T(8,128)(2,1)S(1)} all-reduce(bf16[64,16]{1,0:T(8,128)(2,1)S(1)} %convolution_convert_fusion.6), channel_id=4, replica_groups=mesh['kv'=8,'tp'=4] {'kv'}, use_global_device_ids=true, to_apply=%region_4.5.clone | all-reduce | flops 1024 | bytes 4096
  156.5 0.1 add_rsqrt_fusion.4
  156.7 0.1 add_divide_fusion
  156.8 26.2 %reduce-scatter.5.cloned.1.call-done = bf16[8,3072]{1,0:T(8,128)(2,1)} async-done(((bf16[64,3072]{1,0:T(8,128)(2,1)}), bf16[8,3072]{1,0:T(8,128)(2,1)}) %reduce-scatter.5.cloned.1.call-update) | async-done | bytes 49168 | tf_op jit(solution)/shard_map/reduce_scatter | solution.py:95
  183.0 1.0 convert_multiply_fusion
  184.1 0.1 fusion.42
  184.2 0.1 fusion.43
  184.3 5.8 %fusion = f32[8,8,1,128]{3,2,1,0:T(1,128)S(1)} fusion(f32[8,8,128,1]{2,3,1,0:T(1,128)S(1)} %bitcast.58, f32[8,8,128,128]{3,2,1,0:T(8,128)} %param.22, f32[8,8]{1,0:T(8,128)S(1)} %get-tuple-element.11), kind=kOutput, calls=%fused_computation.1 | convolution fusion | flops 13631488 | bytes 4260096 | tf_op jit(solution)/shard_map/rhab,rha->rhb/dot_general | solution.py:52
  190.1 0.1 fusion.37
  190.2 1.5 multiply_add_fusion
  191.8 2.0 copy-done.2
  193.8 3.6 %fusion.60 = f32[8,8,1,128]{3,2,1,0:T(1,128)S(1)} fusion(f32[8,8,128,128]{3,2,1,0:T(8,128)S(1)} %multiply_add_fusion, f32[8,8,128,1]{2,3,1,0:T(1,128)S(1)} %bitcast.61), kind=kOutput, calls=%fused_computation.97 | convolution fusion | flops 12582912 | bytes 4259840 | tf_op jit(solution)/shard_map/rhab,rha->rhb/dot_general | solution.py:55
  197.5 0.1 fusion.35
  197.6 0.1 fusion.45
  197.7 30.6 %all_gather.16 = bf16[64,1024]{1,0:T(8,128)(2,1)S(1)} all-gather(bf16[8,1024]{1,0:T(8,128)(2,1)S(1)} %fusion.45), channel_id=1, replica_groups=mesh['kv'=8,'tp'=4] {'kv'}, dimensions={0}, use_global_device_ids=true | all-gather | bytes 147456 | tf_op jit(solution)/shard_map/all_gather | solution.py:134
  228.3 0.2 convolution_convert_fusion.4
  228.6 10.3 %psum.38 = bf16[64,256]{1,0:T(8,128)(2,1)S(1)} all-reduce(bf16[64,256]{1,0:T(8,128)(2,1)S(1)} %convolution_convert_fusion.4), channel_id=1, replica_groups=mesh['kv'=8,'tp'=4] {'tp'}, use_global_device_ids=true, to_apply=%region_11.12 | all-reduce | flops 16384 | bytes 65536 | tf_op jit(solution)/shard_map/psum | solution.py:138
  238.9 1.1 convolution_convert_fusion
  240.1 0.1 fusion.32
  240.2 0.2 dynamic-update-slice.1
  240.4 19.7 %all-reduce.1 = bf16[512]{0:T(512)(128)(2,1)S(1)} all-reduce(bf16[512]{0:T(512)(128)(2,1)S(1)} %dynamic-update-slice.1), channel_id=3, replica_groups=mesh['kv'=8,'tp'=4] {'kv'}, use_global_device_ids=true, to_apply=%add.1 | all-reduce | flops 512 | bytes 2048
  260.1 0.1 reshape.88
  260.2 50.7 %all-reduce.8.cloned.1.call-done = bf16[64,2816]{1,0:T(8,128)(2,1)} async-done(((bf16[64,2816]{1,0:T(8,128)(2,1)}), bf16[64,2816]{1,0:T(8,128)(2,1)}) %all-reduce.8.cloned.1.call-update) | async-done | bytes 360464 | tf_op jit(solution)/shard_map/psum | solution.py:25
  311.0 1.0 convert_element_type.150
  312.0 0.3 convolution_convert_fusion.3
  312.3 0.7 copy.43
  313.1 19.0 %reduce-scatter.7.cloned.1.call-done = bf16[64,64]{1,0:T(8,128)(2,1)} async-done(((bf16[256,64]{1,0:T(8,128)(2,1)}), bf16[64,64]{1,0:T(8,128)(2,1)}) %reduce-scatter.7.cloned.1.call-update) | async-done | bytes 8208
  332.0 0.8 copy.44
  332.8 0.7 add_convert_fusion
  (52 shorter events, 0.6 us)
Async XLA Ops:
  7.2 84.4 %copy-start = (bf16[1408,256]{1,0:T(8,128)(2,1)S(1)}, bf16[1408,256]{1,0:T(8,128)(2,1)}, u32[]{:S(2)}) copy-start(bf16[1408,256]{1,0:T(8,128)(2,1)} %param.26) | copy-start | bytes 2162692
  7.2 83.3 %all-reduce.6.cloned.1.call-start = ((), (), s32[]{:S(2)}) async-start(), calls=%async_computation.2 | async-start | bytes 720896 | tf_op jit(solution)/shard_map/psum | solution.py:25
  14.4 107.6 %copy-start.9 = (bf16[256,1024]{1,0:T(8,128)(2,1)S(1)}, bf16[256,1024]{1,0:T(8,128)(2,1)}, u32[]{:S(2)}) copy-start(bf16[256,1024]{1,0:T(8,128)(2,1)} %param.31) | copy-start | bytes 1572868
  14.4 107.6 %copy-start.10 = (bf16[256,1024]{1,0:T(8,128)(2,1)S(1)}, bf16[256,1024]{1,0:T(8,128)(2,1)}, u32[]{:S(2)}) copy-start(bf16[256,1024]{1,0:T(8,128)(2,1)} %param.30) | copy-start | bytes 1572868
  14.4 107.6 %copy-start.11 = (bf16[256,512]{1,0:T(8,128)(2,1)S(1)}, bf16[256,512]{1,0:T(8,128)(2,1)}, u32[]{:S(2)}) copy-start(bf16[256,512]{1,0:T(8,128)(2,1)} %param.29) | copy-start | bytes 786436
  14.4 107.6 %copy-start.12 = (bf16[256,512]{1,0:T(8,128)(2,1)S(1)}, bf16[256,512]{1,0:T(8,128)(2,1)}, u32[]{:S(2)}) copy-start(bf16[256,512]{1,0:T(8,128)(2,1)} %param.28) | copy-start | bytes 786436
  14.4 107.6 %copy-start.13 = (f32[256]{0:T(256)S(1)}, f32[256]{0:T(256)}, u32[]{:S(2)}) copy-start(f32[256]{0:T(256)} %param.27) | copy-start | bytes 3076
  17.0 166.0 %reduce-scatter.5.cloned.1.call-start = ((), (), s32[]{:S(2)}) async-start(), calls=%async_computation.3 | async-start | bytes 442368 | tf_op jit(solution)/shard_map/reduce_scatter | solution.py:95
  91.9 64.8 %copy-start.5 = (f32[8]{0:T(128)S(1)}, f32[8]{0:T(128)}, u32[]{:S(2)}) copy-start(f32[8]{0:T(128)} %param.35) | copy-start | bytes 100
  123.2 187.8 %all-reduce.8.cloned.1.call-start = ((), (), s32[]{:S(2)}) async-start(), calls=%async_computation.4 | async-start | bytes 720896 | tf_op jit(solution)/shard_map/psum | solution.py:25
  183.0 7.2 %copy-start.1 = (f32[8,8,128,128]{3,2,1,0:T(8,128)S(1)}, f32[8,8,128,128]{3,2,1,0:T(8,128)}, u32[]{:S(2)}) copy-start(f32[8,8,128,128]{3,2,1,0:T(8,128)} %param.22) | copy-start | bytes 12582916
  191.7 2.1 copy-start.2
  191.7 5.9 %copy-start.4 = (f32[128]{0:T(128)S(1)}, f32[128]{0:T(128)}, u32[]{:S(2)}) copy-start(f32[128]{0:T(128)} %param.36) | copy-start | bytes 1540
  191.7 36.6 %copy-start.3 = (bf16[1024,256]{1,0:T(8,128)(2,1)S(1)}, bf16[1024,256]{1,0:T(8,128)(2,1)}, u32[]{:S(2)}) copy-start(bf16[1024,256]{1,0:T(8,128)(2,1)} %param.37) | copy-start | bytes 1572868
  191.7 47.1 %copy-start.6 = (bf16[256,1408]{1,0:T(8,128)(2,1)S(1)}, bf16[256,1408]{1,0:T(8,128)(2,1)}, u32[]{:S(2)}) copy-start(bf16[256,1408]{1,0:T(8,128)(2,1)} %param.40) | copy-start | bytes 2162692
  191.8 47.1 %copy-start.7 = (bf16[256,1408]{1,0:T(8,128)(2,1)S(1)}, bf16[256,1408]{1,0:T(8,128)(2,1)}, u32[]{:S(2)}) copy-start(bf16[256,1408]{1,0:T(8,128)(2,1)} %param.39) | copy-start | bytes 2162692
  191.8 47.1 %copy-start.14 = (f32[256]{0:T(256)S(1)}, f32[256]{0:T(256)}, u32[]{:S(2)}) copy-start(f32[256]{0:T(256)} %param.38) | copy-start | bytes 3076
  197.5 114.5 %copy-start.8 = (bf16[1408,256]{1,0:T(8,128)(2,1)S(1)}, bf16[1408,256]{1,0:T(8,128)(2,1)}, u32[]{:S(2)}) copy-start(bf16[1408,256]{1,0:T(8,128)(2,1)} %param.41) | copy-start | bytes 2162692
  240.0 92.0 %reduce-scatter.7.cloned.1.call-start = ((), (), s32[]{:S(2)}) async-start(), calls=%async_computation.5 | async-start | bytes 81920
Sparse Core Ops, SparseCore 0:
  17.1 73.3 all-reduce.5
  123.3 59.6 reduce-scatter.4
  240.1 70.7 all-reduce.7
  313.2 18.7 reduce-scatter.6
